TPU v7x, 32 devices: a whole 2x2x4 slice. The times are simulated.
32 devices in a mesh: sp: 8 (over z, core), tp: 4 (over y, x).
Axes of the slice: x: 2, y: 2, z: 4, core: 2. Of those that a mesh axis runs over, the one named last changes fastest.
Arguments:
- moe_input: bfloat16 [1024, 2048], P('sp', 'tp'), may hold values from -6 to 6
- cotangent: bfloat16 [1024, 2048], P('sp', 'tp'), may hold values from -6 to 6
- routes: int32 [1024, 2], P('sp'), may hold values from 0 to 7, all different within a row; in each aligned block of 128 rows (0 to 127, 128 to 255, ...) at most 64 rows name the same one
- route_weight: float32 [1024, 2], P('sp'), may hold values from 0.1 to 1
- w_gate: bfloat16 [8, 2816, 2048], P('sp', 'tp'), may hold values from -0.125 to 0.125
- w_up: bfloat16 [8, 2816, 2048], P('sp', 'tp'), may hold values from -0.125 to 0.125
- w_down: bfloat16 [8, 2816, 2048], P('sp', 'tp'), may hold values from -0.109375 to 0.109375
- v_value: bfloat16 [1024, 1024], P('sp', 'tp'), may hold values from -6 to 6
- v_gate: bfloat16 [1024, 1024], P('sp', 'tp'), may hold values from -12 to 12
- conv_out: bfloat16 [1024, 1024], P('sp', 'tp'), may hold values from -6 to 6
- row_mean: float32 [1024], P('sp'), may hold values from -3 to 3
- row_rstd: float32 [1024], P('sp'), may hold values from 0.5 to 2
- ln_gain: float32 [1024], P('tp'), may hold values from 0.1 to 1.9
- taps: bfloat16 [31, 1024], P(None, 'tp'), may hold values from -1 to 1
- out_proj: bfloat16 [2048, 1024], P('sp', 'tp'), may hold values from -0.1875 to 0.1875
Outputs:
- gate_grad: bfloat16 [8, 2816, 2048], P('sp', 'tp')
- up_grad: bfloat16 [8, 2816, 2048], P('sp', 'tp')
- down_grad: bfloat16 [8, 2816, 2048], P('sp', 'tp')
- proj_grad: float32 [2048, 1024], P('sp', 'tp')
- stream_grad: bfloat16 [1024, 2048], P('sp', 'tp')
- value_grad: bfloat16 [1024, 1024], P('sp', 'tp')
- gating_grad: bfloat16 [1024, 1024], P('sp', 'tp')
Inputs may be any that keep to these rules, and one draw needn't show every extreme that they name: `routes`: in the rows of one device no expert is named more than 64 times.
All inputs are finite; a program needn't handle non-finite values.
Results may differ from a plain program's by a relative error of at most 0.025.
Values may be sent and summed in bfloat16 or wider, within the bound.
A program may use at most 64 MiB of HBM per device.

v0:
```python
import jax
import jax.numpy as jnp
from jax import lax
from jax.sharding import PartitionSpec as P


def passed_along(value, axis, steps):
    count = lax.axis_size(axis)
    leading, last = (max(0, -steps), min(count, count - steps))
    return lax.ppermute(value, axis, [(source, source + steps) for source in range(leading, last)])


def route_targets(routes, experts, capacity):
    flat_routes = routes.reshape(-1)
    member = (flat_routes[:, None] == jnp.arange(experts, dtype=jnp.int32)[None, :]).astype(
        jnp.int32
    )
    earlier = jnp.cumsum(member, axis=0) - member
    slot_index = jnp.sum(earlier * member, axis=1)
    return flat_routes * capacity + slot_index


def contract_rows(left, right):
    return lax.dot_general(
        left, right, (((0,), (0,)), ((), ())), preferred_element_type=jnp.float32
    )


def contract_cols(left, right):
    return lax.dot_general(
        left, right, (((1,), (1,)), ((), ())), preferred_element_type=jnp.float32
    )


def shards(
    moe_input,
    cotangent,
    routes,
    route_weight,
    w_gate,
    w_up,
    w_down,
    v_value,
    v_gate,
    conv_out,
    row_mean,
    row_rstd,
    ln_gain,
    taps,
    out_proj,
):
    experts = lax.axis_size("sp")
    tokens = routes.shape[0]
    capacity = 4 * tokens // experts
    total = experts * capacity
    buffer_row = route_targets(routes, experts, capacity)
    token_index = jnp.arange(2 * tokens, dtype=jnp.int32) // 2
    weights = route_weight.reshape(-1)
    width = moe_input.shape[1]
    picked = moe_input[token_index]
    weighted = (weights[:, None] * cotangent[token_index].astype(jnp.float32)).astype(jnp.bfloat16)
    rows_buf = jnp.zeros((total, width), jnp.bfloat16).at[buffer_row].set(picked)
    cotan_buf = jnp.zeros((total, width), jnp.bfloat16).at[buffer_row].set(weighted)
    rows_buf, cotan_buf = (
        rows_buf.reshape(experts, capacity, width),
        cotan_buf.reshape(experts, capacity, width),
    )
    part_rows, part_cotan = (
        lax.all_to_all(rows_buf, "sp", split_axis=0, concat_axis=0, tiled=True),
        lax.all_to_all(cotan_buf, "sp", split_axis=0, concat_axis=0, tiled=True),
    )
    arrived_rows, arrived_cotan = (
        lax.all_gather(part_rows, "tp", axis=2, tiled=True),
        lax.all_gather(part_cotan, "tp", axis=2, tiled=True),
    )
    width = arrived_rows.shape[2]
    expert_in = arrived_rows.reshape(total, width)
    expert_cot = arrived_cotan.reshape(total, width)
    gate_w = w_gate[0]
    up_w = w_up[0]
    down_w = w_down[0]
    gate_pre = contract_cols(expert_in, gate_w)
    up_pre = contract_cols(expert_in, up_w)
    gate_sig = jax.nn.sigmoid(gate_pre)
    gate_act = gate_pre * gate_sig
    hidden = (gate_act * up_pre).astype(jnp.bfloat16)
    down_g = contract_rows(hidden, expert_cot).astype(jnp.bfloat16)
    hidden_grad = contract_cols(expert_cot, down_w)
    gate_delta = (hidden_grad * up_pre * gate_sig * (1.0 + gate_pre * (1.0 - gate_sig))).astype(
        jnp.bfloat16
    )
    up_delta = (hidden_grad * gate_act).astype(jnp.bfloat16)
    gate_g = contract_rows(gate_delta, expert_in).astype(jnp.bfloat16)
    up_g = contract_rows(up_delta, expert_in).astype(jnp.bfloat16)
    partial_value = jnp.dot(gate_delta, gate_w, preferred_element_type=jnp.float32) + jnp.dot(
        up_delta, up_w, preferred_element_type=jnp.float32
    )
    row_share = lax.psum_scatter(
        partial_value.astype(jnp.bfloat16), "tp", scatter_dimension=1, tiled=True
    )
    slice_width = row_share.shape[1]
    returned = lax.all_to_all(
        row_share.reshape(experts, capacity, slice_width),
        "sp",
        split_axis=0,
        concat_axis=0,
        tiled=True,
    )
    mine = (
        returned.reshape(total, slice_width)[buffer_row]
        .astype(jnp.float32)
        .reshape(tokens, 2, slice_width)
    )
    stream = (cotangent.astype(jnp.float32) + (mine[:, 0] + mine[:, 1])).astype(jnp.bfloat16)
    full_stream = lax.all_gather(stream, "tp", axis=1, tiled=True)
    normed = (conv_out.astype(jnp.float32) - row_mean[:, None]) * row_rstd[:, None]
    scaled_norm = normed * ln_gain[None, :]
    norm_sig = jax.nn.sigmoid(scaled_norm)
    mixed = (scaled_norm * norm_sig).astype(jnp.bfloat16)
    columns = full_stream
    mixed_grad = jnp.dot(
        columns,
        lax.all_gather(out_proj, "sp", axis=0, tiled=True),
        preferred_element_type=jnp.float32,
    )
    columns = full_stream
    proj_g = lax.psum_scatter(
        contract_rows(columns, mixed).astype(jnp.bfloat16), "sp", scatter_dimension=0, tiled=True
    ).astype(jnp.float32)
    channels = out_proj.shape[1] * lax.axis_size("tp")
    norm_grad = mixed_grad * norm_sig * (1.0 + scaled_norm * (1.0 - norm_sig)) * ln_gain[None, :]
    first_sum, second_sum = lax.psum(
        (jnp.sum(norm_grad, axis=1), jnp.sum(norm_grad * normed, axis=1)), "tp"
    )
    first_mean = first_sum[:, None] / channels
    second_mean = second_sum[:, None] / channels
    conv_grad = row_rstd[:, None] * (norm_grad - first_mean - normed * second_mean)
    kernel = taps.shape[0]
    following = passed_along(conv_grad[: kernel - 1], "sp", -1)
    extended = jnp.concatenate([conv_grad, following], axis=0)
    tap_values = taps.astype(jnp.float32)
    unit_grad = jnp.zeros_like(conv_grad)
    for offset in range(kernel):
        lead = kernel - 1 - offset
        unit_grad = unit_grad + tap_values[offset][None, :] * extended[lead : lead + tokens]
    value_sig = jax.nn.sigmoid(v_gate.astype(jnp.float32))
    value_g = (unit_grad * value_sig).astype(jnp.bfloat16)
    gating_g = (unit_grad * v_value.astype(jnp.float32) * value_sig * (1.0 - value_sig)).astype(
        jnp.bfloat16
    )
    return (gate_g[None], up_g[None], down_g[None], proj_g, stream, value_g, gating_g)


def solution(mesh):
    return jax.shard_map(
        shards,
        mesh=mesh,
        in_specs=(
            P("sp", "tp"),
            P("sp", "tp"),
            P("sp", None),
            P("sp", None),
            P("sp", "tp", None),
            P("sp", "tp", None),
            P("sp", "tp", None),
            P("sp", "tp"),
            P("sp", "tp"),
            P("sp", "tp"),
            P("sp"),
            P("sp"),
            P("tp"),
            P(None, "tp"),
            P("sp", "tp"),
        ),
        out_specs=(
            P("sp", "tp", None),
            P("sp", "tp", None),
            P("sp", "tp", None),
            P("sp", "tp"),
            P("sp", "tp"),
            P("sp", "tp"),
            P("sp", "tp"),
        ),
        check_vma=False,
    )
```

profile of v0, /device:TPU:0, one launch (start us, length us, event | category | flops | bytes accessed | tf_op | source)
XLA Modules:
  0.0 229.9 jit_solution(8924655824834304868)
XLA Ops:
  8.0 0.0 copy-start
  8.0 0.0 copy-start.3
  8.0 0.0 all-gather.6.cloned.1.call-start
  8.1 0.9 copy.25
  9.0 0.1 eq.29
  9.2 0.1 eq.25
  9.3 0.7 broadcast_multiply_fusion
  10.0 0.6 reduce-window.6
  10.6 0.2 slice_reduce_fusion
  10.9 0.1 copy.24
  11.0 0.1 mul.425
  11.1 0.1 fusion.120
  11.2 3.9 %scatter_custom_fusion.1 = bf16[512,512]{1,0:T(8,128)(2,1)S(1)} fusion(s32[256]{0:T(256)S(1)} %bitcast.123, bf16[128,512]{1,0:T(8,128)(2,1)} %param.15, s32[1024]{0:T(1024)S(1)} %pad_clamp_fusion.1, bf16[]{:T(256)} %constant.29.clone.1), kind=kCustom, calls=%fused_computation.94 | custom fusion | bytes 524800 | tf_op jit(solution)/shard_map/scatter | solution.py:62
  15.1 21.6 %all_to_all.15 = bf16[8,64,512]{2,1,0:T(8,128)(2,1)} all-to-all(bf16[8,64,512]{2,1,0:T(8,128)(2,1)S(1)} %bitcast.90), channel_id=1, replica_groups=mesh['sp'=8,'tp'=4] {'sp'}, dimensions={0} | all-to-all | bytes 1048576 | tf_op jit(solution)/shard_map/all_to_all | solution.py:69
  36.7 0.0 all-gather.6.cloned.1.call-update
  36.7 0.0 all-gather.4.cloned.1.call-start
  36.8 0.1 copy.27
  36.9 0.1 mul.427
  37.1 2.9 %scatter_custom_fusion = bf16[512,512]{1,0:T(8,128)(2,1)S(1)} fusion(s32[256]{0:T(256)S(1)} %bitcast.124, f32[256]{0:T(256)S(1)} %mul.427, bf16[]{:T(256)} %constant.29.clone.1, bf16[128,512]{1,0:T(8,128)(2,1)S(1)} %copy-done.3, s32[1024]{0:T(1024)S(1)} %pad_clamp_fusion.1), kind=kCustom, calls=%fused_computation.89 | custom fusion | flops 393216 | bytes 660482 | tf_op jit(solution)/shard_map/scatter | solution.py:63
  39.9 18.4 %all_to_all.16 = bf16[8,64,512]{2,1,0:T(8,128)(2,1)} all-to-all(bf16[8,64,512]{2,1,0:T(8,128)(2,1)S(1)} %bitcast.89), channel_id=1, replica_groups=mesh['sp'=8,'tp'=4] {'sp'}, dimensions={0} | all-to-all | bytes 1048576 | tf_op jit(solution)/shard_map/all_to_all | solution.py:70
  58.4 0.0 all-gather.4.cloned.1.call-update
  58.4 0.2 reduce-scatter.3.cloned.1.call-start
  58.6 12.3 %all-gather.6.cloned.1.call-done = bf16[8,64,2048]{2,1,0:T(8,128)(2,1)} async-done(((bf16[8,64,512]{2,1,0:T(8,128)(2,1)}), bf16[8,64,2048]{2,1,0:T(8,128)(2,1)}) %all-gather.6.cloned.1.call-update) | async-done | bytes 2097168 | tf_op jit(solution)/shard_map/all_gather | solution.py:73
  70.9 4.5 %fusion.5 = f32[512,704]{0,1:T(8,128)} fusion(bf16[512,2048]{1,0:T(8,128)(2,1)} %bitcast.128, bf16[1,704,2048]{2,1,0:T(8,128)(2,1)S(1)} %copy-done), kind=kOutput, calls=%fused_computation.14 | convolution fusion | flops 1476395008 | bytes 6422528 | tf_op jit(solution)/shard_map/dot_general | solution.py:30
  75.4 2.8 %fusion.8 = f32[512,704]{0,1:T(8,128)} fusion(bf16[512,2048]{1,0:T(8,128)(2,1)S(1)} %bitcast.131, bf16[1,704,2048]{2,1,0:T(8,128)(2,1)S(1)} %copy-done.42), kind=kOutput, calls=%fused_computation.17 | convolution fusion | flops 1476395008 | bytes 6422528 | tf_op jit(solution)/shard_map/dot_general | solution.py:30
  78.2 29.5 %all-gather.4.cloned.1.call-done = bf16[8,64,2048]{2,1,0:T(8,128)(2,1)} async-done(((bf16[8,64,512]{2,1,0:T(8,128)(2,1)}), bf16[8,64,2048]{2,1,0:T(8,128)(2,1)}) %all-gather.4.cloned.1.call-update) | async-done | bytes 2097168 | tf_op jit(solution)/shard_map/all_gather | solution.py:74
  107.8 5.4 %multiply_convert_fusion.1 = (bf16[512,704]{0,1:T(8,128)(2,1)S(1)}, bf16[512,704]{0,1:T(8,128)(2,1)S(1)}) fusion(f32[512,704]{0,1:T(8,128)} %fusion.5, f32[512,704]{0,1:T(8,128)} %fusion.8, bf16[512,2048]{1,0:T(8,128)(2,1)} %bitcast.132, bf16[1,704,2048]{2,1,0:T(8,128)(2,1)} %param.21), kind=kOutput, calls=%fused_computation.52 | convolution fusion | flops 1481080832 | bytes 9306112 | tf_op jit(solution)/shard_map/dot_general | solution.py:30
  113.2 0.0 copy-start.43
  113.2 1.9 fusion.3
  115.1 0.4 copy-done.43
  115.5 3.3 %add_convert_fusion = bf16[512,2048]{1,0:T(8,128)(2,1)} fusion(f32[512,2048]{1,0:T(8,128)S(1)} %fusion.3, bf16[512,704]{0,1:T(8,128)(2,1)S(1)} %get-tuple-element.13, bf16[1,704,2048]{2,1,0:T(8,128)(2,1)S(1)} %copy-done.43), kind=kOutput, calls=%fused_computation.5 | convolution fusion | flops 1478492160 | bytes 9895936 | tf_op jit(solution)/shard_map/dot_general | solution.py:95
  118.8 0.0 reduce-scatter.3.cloned.1.call-update
  118.8 0.0 all-gather.8.cloned.1.call-start
  118.9 0.5 all-gather.8.cloned.1.call-update
  119.4 34.8 %reduce-scatter.3.cloned.1.call-done = bf16[512,512]{1,0:T(8,128)(2,1)} async-done(((bf16[512,2048]{1,0:T(8,128)(2,1)}), bf16[512,512]{1,0:T(8,128)(2,1)}) %reduce-scatter.3.cloned.1.call-update) | async-done | bytes 524304 | tf_op jit(solution)/shard_map/reduce_scatter | solution.py:98
  154.2 4.6 %all-to-all-start.2 = ((bf16[8,64,512]{2,1,0:T(8,128)(2,1)}), bf16[8,64,512]{2,1,0:T(8,128)(2,1)S(1)}, u32[]{:S(2)}, u32[]{:S(2)}) async-start(bf16[8,64,512]{2,1,0:T(8,128)(2,1)} %bitcast.91), calls=%async_computation.3 | async-start | bytes 1048576 | tf_op jit(solution)/shard_map/all_to_all | solution.py:102
  158.8 0.0 reduce-scatter.5.cloned.1.call-start
  158.9 0.6 fusion.129
  159.5 0.7 fusion.128
  160.2 5.1 %fusion.1 = bf16[1,704,2048]{2,1,0:T(8,128)(2,1)} fusion(bf16[512,704]{0,1:T(8,128)(2,1)} %copy-done.45, bf16[512,2048]{1,0:T(8,128)(2,1)} %bitcast.129), kind=kOutput, calls=%fused_computation.10 | convolution fusion | flops 1477836800 | bytes 5701632 | tf_op jit(solution)/shard_map/dot_general | solution.py:24
  165.2 8.9 %all-to-all-done.2 = bf16[8,64,512]{2,1,0:T(8,128)(2,1)S(1)} async-done(((bf16[8,64,512]{2,1,0:T(8,128)(2,1)}), bf16[8,64,512]{2,1,0:T(8,128)(2,1)S(1)}, u32[]{:S(2)}, u32[]{:S(2)}) %all-to-all-start.2) | async-done | bytes 524320 | tf_op jit(solution)/shard_map/all_to_all | solution.py:102
  174.1 1.9 gather_fusion
  176.0 1.3 reshape.141
  177.3 0.0 copy-start.4
  177.3 0.0 copy-start.36
  177.3 0.0 copy-start.38
  177.3 0.4 fusion.127
  177.7 1.0 fusion.18
  178.7 0.0 copy-start.2
  178.7 10.5 %all_gather.14 = bf16[128,2048]{1,0:T(8,128)(2,1)S(1)} all-gather(bf16[128,512]{1,0:T(8,128)(2,1)S(1)} %fusion.18), channel_id=1, replica_groups=mesh['sp'=8,'tp'=4] {'tp'}, dimensions={1}, use_global_device_ids=true | all-gather | bytes 655360 | tf_op jit(solution)/shard_map/all_gather | solution.py:115
  189.2 1.6 convolution_convert_fusion.3
  190.8 0.0 reduce-scatter.5.cloned.1.call-update
  190.8 5.7 %fusion.2 = bf16[1,704,2048]{2,1,0:T(8,128)(2,1)} fusion(bf16[512,2048]{1,0:T(8,128)(2,1)} %bitcast.133, f32[512,704]{0,1:T(8,128)} %fusion.8, f32[512,704]{0,1:T(8,128)} %fusion.5), kind=kOutput, calls=%fused_computation.11 | convolution fusion | flops 1479999488 | bytes 7864320 | tf_op jit(solution)/shard_map/dot_general | solution.py:24
  196.6 2.3 fusion.125
  198.9 8.9 %all-reduce = (f32[128]{0:T(128)S(1)}, f32[128]{0:T(128)S(1)}) all-reduce(f32[128]{0:T(128)S(1)} %get-tuple-element.8, f32[128]{0:T(128)S(1)} %get-tuple-element.7), channel_id=1, replica_groups=mesh['sp'=8,'tp'=4] {'tp'}, use_global_device_ids=true, to_apply=%region_10.11 | all-reduce | flops 256 | bytes 2048 | tf_op jit(solution)/shard_map/psum | solution.py:132
  207.8 1.0 subtract_multiply_fusion
  208.9 0.0 copy-start.7
  208.9 0.0 copy-start.9
  209.2 1.3 collective-permute-start
  210.5 5.1 %fusion = bf16[1,704,2048]{2,1,0:T(8,128)(2,1)} fusion(bf16[512,704]{0,1:T(8,128)(2,1)} %copy-done.1, bf16[512,2048]{1,0:T(8,128)(2,1)} %bitcast.130), kind=kOutput, calls=%fused_computation.9 | convolution fusion | flops 1477836800 | bytes 5701632 | tf_op jit(solution)/shard_map/dot_general | solution.py:24
  215.8 1.1 multiply_convert_fusion.6
  217.0 0.7 multiply_convert_fusion.7
  217.6 3.5 %reduce-scatter.5.cloned.1.call-done = bf16[256,256]{1,0:T(8,128)(2,1)} async-done(((bf16[2048,256]{1,0:T(8,128)(2,1)}), bf16[256,256]{1,0:T(8,128)(2,1)}) %reduce-scatter.5.cloned.1.call-update) | async-done | bytes 131088 | tf_op jit(solution)/shard_map/reduce_scatter | solution.py:127
  221.1 1.6 convert_element_type.92
  (93 shorter events, 0.3 us)
Async XLA Ops:
  8.0 62.9 %copy-start = (bf16[1,704,2048]{2,1,0:T(8,128)(2,1)S(1)}, bf16[1,704,2048]{2,1,0:T(8,128)(2,1)}, u32[]{:S(2)}) copy-start(bf16[1,704,2048]{2,1,0:T(8,128)(2,1)} %param.19) | copy-start | bytes 8650756
  8.0 28.8 %copy-start.40 = (f32[128,2]{0,1:T(2,128)S(1)}, f32[128,2]{0,1:T(2,128)}, u32[]{:S(2)}) copy-start(f32[128,2]{0,1:T(2,128)} %param.18) | copy-start | bytes 3076
  8.0 29.0 %copy-start.3 = (bf16[128,512]{1,0:T(8,128)(2,1)S(1)}, bf16[128,512]{1,0:T(8,128)(2,1)}, u32[]{:S(2)}) copy-start(bf16[128,512]{1,0:T(8,128)(2,1)} %param.16) | copy-start | bytes 393220
  8.0 62.8 %all-gather.6.cloned.1.call-start = ((), (), s32[]{:S(2)}) async-start(), calls=%async_computation.6 | async-start | bytes 2621440 | tf_op jit(solution)/shard_map/all_gather | solution.py:73
  36.7 71.0 %all-gather.4.cloned.1.call-start = ((), (), s32[]{:S(2)}) async-start(), calls=%async_computation.5 | async-start | bytes 2621440 | tf_op jit(solution)/shard_map/all_gather | solution.py:74
  58.4 95.8 %reduce-scatter.3.cloned.1.call-start = ((), (), s32[]{:S(2)}) async-start(), calls=%async_computation.7 | async-start | bytes 2621440 | tf_op jit(solution)/shard_map/reduce_scatter | solution.py:98
  70.9 4.5 %copy-start.42 = (bf16[1,704,2048]{2,1,0:T(8,128)(2,1)S(1)}, bf16[1,704,2048]{2,1,0:T(8,128)(2,1)}, u32[]{:S(2)}) copy-start(bf16[1,704,2048]{2,1,0:T(8,128)(2,1)} %param.20) | copy-start | bytes 8650756
  70.9 4.5 %copy-start.44 = (bf16[8,64,2048]{2,1,0:T(8,128)(2,1)S(1)}, bf16[8,64,2048]{2,1,0:T(8,128)(2,1)}, u32[]{:S(2)}) copy-start(bf16[8,64,2048]{2,1,0:T(8,128)(2,1)} %all-gather.6.cloned.1.call-done) | copy-start | bytes 6291460
  113.1 1.9 copy-start.1
  113.2 1.9 copy-start.45
  113.2 2.3 %copy-start.43 = (bf16[1,704,2048]{2,1,0:T(8,128)(2,1)S(1)}, bf16[1,704,2048]{2,1,0:T(8,128)(2,1)}, u32[]{:S(2)}) copy-start(bf16[1,704,2048]{2,1,0:T(8,128)(2,1)} %param.20) | copy-start | bytes 8650756
  118.8 40.0 %copy-start.8 = (bf16[31,256]{1,0:T(8,128)(2,1)S(1)}, bf16[31,256]{1,0:T(8,128)(2,1)}, u32[]{:S(2)}) copy-start(bf16[31,256]{1,0:T(8,128)(2,1)} %param.28) | copy-start | bytes 47620
  118.8 77.7 %all-gather.8.cloned.1.call-start = ((), (), s32[]{:S(2)}) async-start(), calls=%async_computation.9 | async-start | bytes 1179648 | tf_op jit(solution)/shard_map/all_gather | solution.py:123
  154.2 19.9 %all-to-all-start.2 = ((bf16[8,64,512]{2,1,0:T(8,128)(2,1)}), bf16[8,64,512]{2,1,0:T(8,128)(2,1)S(1)}, u32[]{:S(2)}, u32[]{:S(2)}) async-start(bf16[8,64,512]{2,1,0:T(8,128)(2,1)} %bitcast.91), calls=%async_computation.3 | async-start | bytes 1048576 | tf_op jit(solution)/shard_map/all_to_all | solution.py:102
  158.8 62.3 %reduce-scatter.5.cloned.1.call-start = ((), (), s32[]{:S(2)}) async-start(), calls=%async_computation.8 | async-start | bytes 1179648 | tf_op jit(solution)/shard_map/reduce_scatter | solution.py:127
  177.3 11.9 %copy-start.4 = (bf16[128,256]{1,0:T(8,128)(2,1)S(1)}, bf16[128,256]{1,0:T(8,128)(2,1)}, u32[]{:S(2)}) copy-start(bf16[128,256]{1,0:T(8,128)(2,1)} %param.24) | copy-start | bytes 196612
  177.3 11.9 %copy-start.36 = (f32[128]{0:T(128)S(1)}, f32[128]{0:T(128)}, u32[]{:S(2)}) copy-start(f32[128]{0:T(128)} %param.26) | copy-start | bytes 1540
  177.3 11.9 %copy-start.38 = (f32[128]{0:T(128)S(1)}, f32[128]{0:T(128)}, u32[]{:S(2)}) copy-start(f32[128]{0:T(128)} %param.25) | copy-start | bytes 1540
  177.3 11.9 %copy-start.41 = (f32[256]{0:T(256)S(1)}, f32[256]{0:T(256)}, u32[]{:S(2)}) copy-start(f32[256]{0:T(256)} %param.27) | copy-start | bytes 3076
  178.7 17.9 %copy-start.2 = (bf16[128,512]{1,0:T(8,128)(2,1)}, bf16[128,512]{1,0:T(8,128)(2,1)S(1)}, u32[]{:S(2)}) copy-start(bf16[128,512]{1,0:T(8,128)(2,1)S(1)} %fusion.18) | copy-start | bytes 393220
  196.6 11.2 %copy-start.5 = (bf16[128,256]{1,0:T(8,128)(2,1)S(1)}, bf16[128,256]{1,0:T(8,128)(2,1)}, u32[]{:S(2)}) copy-start(bf16[128,256]{1,0:T(8,128)(2,1)} %param.24) | copy-start | bytes 196612
  196.6 11.2 %copy-start.37 = (f32[128]{0:T(128)S(1)}, f32[128]{0:T(128)}, u32[]{:S(2)}) copy-start(f32[128]{0:T(128)} %param.26) | copy-start | bytes 1540
  196.6 11.2 %copy-start.39 = (f32[128]{0:T(128)S(1)}, f32[128]{0:T(128)}, u32[]{:S(2)}) copy-start(f32[128]{0:T(128)} %param.25) | copy-start | bytes 1540
  208.9 6.7 %copy-start.6 = (bf16[128,256]{1,0:T(8,128)(2,1)S(1)}, bf16[128,256]{1,0:T(8,128)(2,1)}, u32[]{:S(2)}) copy-start(bf16[128,256]{1,0:T(8,128)(2,1)} %param.23) | copy-start | bytes 196612
  208.9 6.7 %copy-start.7 = (bf16[128,256]{1,0:T(8,128)(2,1)S(1)}, bf16[128,256]{1,0:T(8,128)(2,1)}, u32[]{:S(2)}) copy-start(bf16[128,256]{1,0:T(8,128)(2,1)} %param.22) | copy-start | bytes 196612
  208.9 6.7 %copy-start.9 = (f32[1,256]{1,0:T(1,128)S(1)}, f32[1,256]{1,0:T(1,128)}, u32[]{:S(2)}) copy-start(f32[1,256]{1,0:T(1,128)} %get-tuple-element.40) | copy-start | bytes 3076
  208.9 6.7 %copy-start.10 = (f32[1,256]{1,0:T(1,128)S(1)}, f32[1,256]{1,0:T(1,128)}, u32[]{:S(2)}) copy-start(f32[1,256]{1,0:T(1,128)} %get-tuple-element.41) | copy-start | bytes 3076
  208.9 6.6 %copy-start.11 = (f32[1,256]{1,0:T(1,128)S(1)}, f32[1,256]{1,0:T(1,128)}, u32[]{:S(2)}) copy-start(f32[1,256]{1,0:T(1,128)} %get-tuple-element.42) | copy-start | bytes 3076
  208.9 6.6 %copy-start.12 = (f32[1,256]{1,0:T(1,128)S(1)}, f32[1,256]{1,0:T(1,128)}, u32[]{:S(2)}) copy-start(f32[1,256]{1,0:T(1,128)} %get-tuple-element.43) | copy-start | bytes 3076
  208.9 6.6 %copy-start.13 = (f32[1,256]{1,0:T(1,128)S(1)}, f32[1,256]{1,0:T(1,128)}, u32[]{:S(2)}) copy-start(f32[1,256]{1,0:T(1,128)} %get-tuple-element.44) | copy-start | bytes 3076
  208.9 6.6 %copy-start.14 = (f32[1,256]{1,0:T(1,128)S(1)}, f32[1,256]{1,0:T(1,128)}, u32[]{:S(2)}) copy-start(f32[1,256]{1,0:T(1,128)} %get-tuple-element.45) | copy-start | bytes 3076
  209.0 6.6 %copy-start.15 = (f32[1,256]{1,0:T(1,128)S(1)}, f32[1,256]{1,0:T(1,128)}, u32[]{:S(2)}) copy-start(f32[1,256]{1,0:T(1,128)} %get-tuple-element.46) | copy-start | bytes 3076
  209.0 6.6 %copy-start.16 = (f32[1,256]{1,0:T(1,128)S(1)}, f32[1,256]{1,0:T(1,128)}, u32[]{:S(2)}) copy-start(f32[1,256]{1,0:T(1,128)} %get-tuple-element.47) | copy-start | bytes 3076
  209.0 6.6 %copy-start.17 = (f32[1,256]{1,0:T(1,128)S(1)}, f32[1,256]{1,0:T(1,128)}, u32[]{:S(2)}) copy-start(f32[1,256]{1,0:T(1,128)} %get-tuple-element.17) | copy-start | bytes 3076
  209.0 6.6 %copy-start.18 = (f32[1,256]{1,0:T(1,128)S(1)}, f32[1,256]{1,0:T(1,128)}, u32[]{:S(2)}) copy-start(f32[1,256]{1,0:T(1,128)} %get-tuple-element.18) | copy-start | bytes 3076
  209.0 6.6 %copy-start.19 = (f32[1,256]{1,0:T(1,128)S(1)}, f32[1,256]{1,0:T(1,128)}, u32[]{:S(2)}) copy-start(f32[1,256]{1,0:T(1,128)} %get-tuple-element.19) | copy-start | bytes 3076
  209.0 6.6 %copy-start.20 = (f32[1,256]{1,0:T(1,128)S(1)}, f32[1,256]{1,0:T(1,128)}, u32[]{:S(2)}) copy-start(f32[1,256]{1,0:T(1,128)} %get-tuple-element.20) | copy-start | bytes 3076
  209.0 6.6 %copy-start.21 = (f32[1,256]{1,0:T(1,128)S(1)}, f32[1,256]{1,0:T(1,128)}, u32[]{:S(2)}) copy-start(f32[1,256]{1,0:T(1,128)} %get-tuple-element.21) | copy-start | bytes 3076
  209.0 6.6 %copy-start.22 = (f32[1,256]{1,0:T(1,128)S(1)}, f32[1,256]{1,0:T(1,128)}, u32[]{:S(2)}) copy-start(f32[1,256]{1,0:T(1,128)} %get-tuple-element.22) | copy-start | bytes 3076
  209.0 6.6 %copy-start.23 = (f32[1,256]{1,0:T(1,128)S(1)}, f32[1,256]{1,0:T(1,128)}, u32[]{:S(2)}) copy-start(f32[1,256]{1,0:T(1,128)} %get-tuple-element.23) | copy-start | bytes 3076
  209.0 6.6 %copy-start.24 = (f32[1,256]{1,0:T(1,128)S(1)}, f32[1,256]{1,0:T(1,128)}, u32[]{:S(2)}) copy-start(f32[1,256]{1,0:T(1,128)} %get-tuple-element.24) | copy-start | bytes 3076
  209.1 6.6 %copy-start.25 = (f32[1,256]{1,0:T(1,128)S(1)}, f32[1,256]{1,0:T(1,128)}, u32[]{:S(2)}) copy-start(f32[1,256]{1,0:T(1,128)} %get-tuple-element.25) | copy-start | bytes 3076
  209.1 6.6 %copy-start.26 = (f32[1,256]{1,0:T(1,128)S(1)}, f32[1,256]{1,0:T(1,128)}, u32[]{:S(2)}) copy-start(f32[1,256]{1,0:T(1,128)} %get-tuple-element.26) | copy-start | bytes 3076
  209.1 6.6 %copy-start.27 = (f32[1,256]{1,0:T(1,128)S(1)}, f32[1,256]{1,0:T(1,128)}, u32[]{:S(2)}) copy-start(f32[1,256]{1,0:T(1,128)} %get-tuple-element.27) | copy-start | bytes 3076
  209.1 6.6 %copy-start.28 = (f32[1,256]{1,0:T(1,128)S(1)}, f32[1,256]{1,0:T(1,128)}, u32[]{:S(2)}) copy-start(f32[1,256]{1,0:T(1,128)} %get-tuple-element.28) | copy-start | bytes 3076
  209.1 6.6 %copy-start.29 = (f32[1,256]{1,0:T(1,128)S(1)}, f32[1,256]{1,0:T(1,128)}, u32[]{:S(2)}) copy-start(f32[1,256]{1,0:T(1,128)} %get-tuple-element.29) | copy-start | bytes 3076
  209.1 6.6 %copy-start.30 = (f32[1,256]{1,0:T(1,128)S(1)}, f32[1,256]{1,0:T(1,128)}, u32[]{:S(2)}) copy-start(f32[1,256]{1,0:T(1,128)} %get-tuple-element.30) | copy-start | bytes 3076
  209.1 6.6 %copy-start.31 = (f32[1,256]{1,0:T(1,128)S(1)}, f32[1,256]{1,0:T(1,128)}, u32[]{:S(2)}) copy-start(f32[1,256]{1,0:T(1,128)} %get-tuple-element.31) | copy-start | bytes 3076
  209.1 6.6 %copy-start.32 = (f32[1,256]{1,0:T(1,128)S(1)}, f32[1,256]{1,0:T(1,128)}, u32[]{:S(2)}) copy-start(f32[1,256]{1,0:T(1,128)} %get-tuple-element.32) | copy-start | bytes 3076
  209.1 6.6 %copy-start.33 = (f32[1,256]{1,0:T(1,128)S(1)}, f32[1,256]{1,0:T(1,128)}, u32[]{:S(2)}) copy-start(f32[1,256]{1,0:T(1,128)} %get-tuple-element.33) | copy-start | bytes 3076
  209.1 6.6 %copy-start.34 = (f32[1,256]{1,0:T(1,128)S(1)}, f32[1,256]{1,0:T(1,128)}, u32[]{:S(2)}) copy-start(f32[1,256]{1,0:T(1,128)} %get-tuple-element.34) | copy-start | bytes 3076
  209.2 6.6 %copy-start.35 = (f32[1,256]{1,0:T(1,128)S(1)}, f32[1,256]{1,0:T(1,128)}, u32[]{:S(2)}) copy-start(f32[1,256]{1,0:T(1,128)} %get-tuple-element.35) | copy-start | bytes 3076
  209.2 6.4 %collective-permute-start = (f32[30,256]{1,0:T(8,128)S(1)}, f32[30,256]{1,0:T(8,128)S(1)}, u32[]{:S(2)}, u32[]{:S(2)}) collective-permute-start(f32[30,256]{1,0:T(8,128)S(1)} %slice.274), channel_id=1, source_target_pairs={{4,0},{8,4},{12,8},{16,12},{20,16},{24,20},{28,24},{5,1},{9,5},{13... | collective-permute-start | bytes 92168 | tf_op jit(solution)/shard_map/ppermute | solution.py:10
Sparse Core Ops, SparseCore 0:
  36.9 33.9 all-gather.5
  72.7 35.0 all-gather.3
  119.0 35.1 reduce-scatter.2
Sparse Core Ops, SparseCore 1:
  120.9 22.1 all-gather.7
  190.9 30.2 reduce-scatter.4
where the time goes:
time: 231 us; the launch traced here: 230 us
  waiting for transfers between devices  89.5 us (39%)
  blocking collectives  59.4 us (26%)
  matrix products  37.7 us (16%)
  between operations  15.9 us (7%)
  local copies, waits for them, and re-layouts  11.3 us (5%)
  other arithmetic  9.76 us (4%)
  starting transfers between devices  6.28 us (3%)
    reduce_scatter x1, waiting for transfers between devices, shards(): lax.psum_scatter(partial_value.astype(jnp.bfloat16), 'tp', scatter_dimens...  34.8 us
    all_gather x1, waiting for transfers between devices, shards(): lax.all_gather(part_cotan, 'tp', axis=2, tiled=True)  29.5 us
    all_to_all x1, blocking collectives, shards(): lax.all_to_all(rows_buf, 'sp', split_axis=0, concat_axis=0, tiled=True)  21.6 us
    all_to_all x1, blocking collectives, shards(): lax.all_to_all(cotan_buf, 'sp', split_axis=0, concat_axis=0, tiled=True)  18.4 us
    dot_general x4, matrix products, contract_rows(): lax.dot_general(left, right, (((0,), (0,)), ((), ())), preferred_element_...  17.5 us
    dot_general x3, matrix products, contract_cols(): lax.dot_general(left, right, (((1,), (1,)), ((), ())), preferred_element_...  12.7 us
    all_gather x1, waiting for transfers between devices, shards(): lax.all_gather(part_rows, 'tp', axis=2, tiled=True)  12.3 us
    all_gather x1, blocking collectives, shards(): full_stream = lax.all_gather(stream, 'tp', axis=1, tiled=True)  10.5 us
  transfers between devices with their start and end apart: 7, of which 5 were waited for; matrix products, arithmetic and copies ran while one was open for 17% of the time, Pallas kernels for 0%

commit v1 on v0

--- a/solution.py
+++ b/solution.py
@@ -71,7 +71,9 @@
     )
     arrived_rows, arrived_cotan = (
         lax.all_gather(part_rows, "tp", axis=2, tiled=True),
-        lax.all_gather(part_cotan, "tp", axis=2, tiled=True),
+        jnp.concatenate(
+            lax.all_to_all(jnp.stack([part_cotan] * lax.axis_size("tp")), "tp", 0, 0), axis=2
+        ),
     )
     width = arrived_rows.shape[2]
     expert_in = arrived_rows.reshape(total, width)

time: 231 us -> 223 us (0.965)
  waiting for transfers between devices: 89.5 us -> 47.1 us
  blocking collectives: 59.4 us -> 94.2 us
  matrix products: 37.7 us -> 32.2 us
  local copies, waits for them, and re-layouts: 11.3 us -> 16.4 us
    all_to_all x0 -> x1, blocking collectives: none -> 35.7 us  [shards(): lax.all_to_all(jnp.stack([part_cotan] * lax.axis_size('tp')), 'tp', 0, 0)]
    all_gather x1 -> x0, waiting for transfers between devices: 29.5 us -> none  [shards(): lax.all_gather(part_cotan, 'tp', axis=2, tiled=True)]
    all_gather x1, waiting for transfers between devices: 12.3 us -> 0.01 us  [shards(): lax.all_gather(part_rows, 'tp', axis=2, tiled=True)]
    dot_general x3, matrix products: 12.7 us -> 7.24 us  [contract_cols(): lax.dot_general(left, right, (((1,), (1,)), ((), ())), preferred_element_...]
    unnamed x94 -> x101, local copies, waits for them, and re-layouts: 1.69 us -> 4.98 us
  transfers between devices with their start and end apart: 7 -> 6, of which waited for: 5 -> 3; matrix products, arithmetic and copies ran while one was open for 17% -> 16% of each run, Pallas kernels for 0% -> 0%
where the time goes in v1:
time: 223 us; the launch traced here: 222 us
  blocking collectives  94.2 us (42%)
  waiting for transfers between devices  47.1 us (21%)
  matrix products  32.2 us (14%)
  local copies, waits for them, and re-layouts  16.4 us (7%)
  between operations  16.3 us (7%)
  other arithmetic  9.76 us (4%)
  starting transfers between devices  6.26 us (3%)
    all_to_all x1, blocking collectives, shards(): lax.all_to_all(jnp.stack([part_cotan] * lax.axis_size('tp')), 'tp', 0, 0)  35.7 us
    reduce_scatter x1, waiting for transfers between devices, shards(): lax.psum_scatter(partial_value.astype(jnp.bfloat16), 'tp', scatter_dimens...  34.2 us
    all_to_all x1, blocking collectives, shards(): lax.all_to_all(rows_buf, 'sp', split_axis=0, concat_axis=0, tiled=True)  21.6 us
    all_to_all x1, blocking collectives, shards(): lax.all_to_all(cotan_buf, 'sp', split_axis=0, concat_axis=0, tiled=True)  17.7 us
    dot_general x4, matrix products, contract_rows(): lax.dot_general(left, right, (((0,), (0,)), ((), ())), preferred_element_...  17.5 us
    all_gather x1, blocking collectives, shards(): full_stream = lax.all_gather(stream, 'tp', axis=1, tiled=True)  10.2 us
    psum x1, blocking collectives, shards(): lax.psum((jnp.sum(norm_grad, axis=1), jnp.sum(norm_grad * normed, axis=1)...  8.9 us
    all_to_all x1, waiting for transfers between devices, shards(): lax.all_to_all(row_share.reshape(experts, capacity, slice_width), 'sp', s...  8.7 us
  transfers between devices with their start and end apart: 6, of which 3 were waited for; matrix products, arithmetic and copies ran while one was open for 16% of the time, Pallas kernels for 0%

profile of v1, /device:TPU:0, one launch (start us, length us, event | category | flops | bytes accessed | tf_op | source)
XLA Modules:
  0.0 222.2 jit_solution(2536029228179971361)
XLA Ops:
  8.0 0.0 copy-start
  8.0 0.0 copy-start.4
  8.0 0.0 all-gather.3.cloned.1.call-start
  8.1 0.9 copy.31
  9.0 0.1 eq.29
  9.2 0.1 eq.25
  9.3 0.7 broadcast_multiply_fusion
  10.0 0.6 reduce-window.6
  10.6 0.2 slice_reduce_fusion
  10.9 0.1 copy.30
  11.0 0.1 mul.425
  11.1 0.1 fusion.120
  11.2 3.9 %scatter_custom_fusion.1 = bf16[512,512]{1,0:T(8,128)(2,1)S(1)} fusion(s32[256]{0:T(256)S(1)} %bitcast.130, bf16[128,512]{1,0:T(8,128)(2,1)} %param.15, s32[1024]{0:T(1024)S(1)} %pad_clamp_fusion.1, bf16[]{:T(256)} %constant.29.clone.1), kind=kCustom, calls=%fused_computation.94 | custom fusion | bytes 524800 | tf_op jit(solution)/shard_map/scatter | solution.py:62
  15.1 21.6 %all_to_all.20 = bf16[8,64,512]{2,1,0:T(8,128)(2,1)} all-to-all(bf16[8,64,512]{2,1,0:T(8,128)(2,1)S(1)} %bitcast.97), channel_id=1, replica_groups=mesh['sp'=8,'tp'=4] {'sp'}, dimensions={0} | all-to-all | bytes 1048576 | tf_op jit(solution)/shard_map/all_to_all | solution.py:69
  36.7 0.0 all-gather.3.cloned.1.call-update
  36.7 0.0 reduce-scatter.3.cloned.1.call-start
  36.8 0.1 copy.33
  36.9 0.1 mul.427
  37.1 2.9 %scatter_custom_fusion = bf16[512,512]{1,0:T(8,128)(2,1)S(1)} fusion(s32[256]{0:T(256)S(1)} %bitcast.131, f32[256]{0:T(256)S(1)} %mul.427, bf16[]{:T(256)} %constant.29.clone.1, bf16[128,512]{1,0:T(8,128)(2,1)S(1)} %copy-done.4, s32[1024]{0:T(1024)S(1)} %pad_clamp_fusion.1), kind=kCustom, calls=%fused_computation.89 | custom fusion | flops 393216 | bytes 660482 | tf_op jit(solution)/shard_map/scatter | solution.py:63
  39.9 17.7 %all_to_all.21 = bf16[8,64,512]{2,1,0:T(8,128)(2,1)S(1)} all-to-all(bf16[8,64,512]{2,1,0:T(8,128)(2,1)S(1)} %bitcast.96), channel_id=1, replica_groups=mesh['sp'=8,'tp'=4] {'sp'}, dimensions={0} | all-to-all | bytes 1048576 | tf_op jit(solution)/shard_map/all_to_all | solution.py:70
  57.7 0.2 stack.2
  57.9 35.7 %all_to_all.22 = bf16[4,8,64,512]{3,2,1,0:T(8,128)(2,1)S(1)} all-to-all(bf16[4,8,64,512]{3,2,1,0:T(8,128)(2,1)S(1)} %stack.2), channel_id=1, replica_groups=mesh['sp'=8,'tp'=4] {'tp'}, dimensions={0} | all-to-all | bytes 4194304 | tf_op jit(solution)/shard_map/all_to_all | solution.py:75
  93.7 1.6 copy.34
  95.3 1.9 copy.39
  97.3 3.4 %fusion.5 = f32[512,704]{0,1:T(8,128)S(1)} fusion(bf16[512,2048]{1,0:T(8,128)(2,1)} %bitcast.135, bf16[1,704,2048]{2,1,0:T(8,128)(2,1)S(1)} %copy-done), kind=kOutput, calls=%fused_computation.14 | convolution fusion | flops 1476395008 | bytes 6422528 | tf_op jit(solution)/shard_map/dot_general | solution.py:30
  100.7 0.0 copy-start.1
  100.8 1.7 fusion.8
  102.5 0.4 copy-done.1
  102.8 1.4 copy-done.43
  104.2 2.1 multiply_convert_fusion.1
  106.4 1.9 fusion.3
  108.3 3.3 %add_convert_fusion = bf16[512,2048]{1,0:T(8,128)(2,1)} fusion(f32[512,2048]{1,0:T(8,128)S(1)} %fusion.3, bf16[512,704]{0,1:T(8,128)(2,1)S(1)} %get-tuple-element.13, bf16[1,704,2048]{2,1,0:T(8,128)(2,1)S(1)} %copy-done.44), kind=kOutput, calls=%fused_computation.5 | convolution fusion | flops 1478492160 | bytes 9895936 | tf_op jit(solution)/shard_map/dot_general | solution.py:97
  111.6 0.0 reduce-scatter.3.cloned.1.call-update
  111.6 0.0 all-gather.5.cloned.1.call-start
  111.7 0.5 all-gather.5.cloned.1.call-update
  112.2 34.2 %reduce-scatter.3.cloned.1.call-done = bf16[512,512]{1,0:T(8,128)(2,1)} async-done(((bf16[512,2048]{1,0:T(8,128)(2,1)}), bf16[512,512]{1,0:T(8,128)(2,1)}) %reduce-scatter.3.cloned.1.call-update) | async-done | bytes 524304 | tf_op jit(solution)/shard_map/reduce_scatter | solution.py:100
  146.4 4.6 %all-to-all-start.3 = ((bf16[8,64,512]{2,1,0:T(8,128)(2,1)}), bf16[8,64,512]{2,1,0:T(8,128)(2,1)S(1)}, u32[]{:S(2)}, u32[]{:S(2)}) async-start(bf16[8,64,512]{2,1,0:T(8,128)(2,1)} %bitcast.98), calls=%async_computation.4 | async-start | bytes 1048576 | tf_op jit(solution)/shard_map/all_to_all | solution.py:104
  151.0 0.3 reduce-scatter.5.cloned.1.call-start
  151.3 0.6 fusion.129
  151.9 0.7 fusion.128
  152.6 5.1 %fusion.1 = bf16[1,704,2048]{2,1,0:T(8,128)(2,1)} fusion(bf16[512,704]{0,1:T(8,128)(2,1)} %copy-done.46, bf16[512,2048]{1,0:T(8,128)(2,1)} %bitcast.136), kind=kOutput, calls=%fused_computation.10 | convolution fusion | flops 1477836800 | bytes 5701632 | tf_op jit(solution)/shard_map/dot_general | solution.py:24
  157.6 8.7 %all-to-all-done.3 = bf16[8,64,512]{2,1,0:T(8,128)(2,1)S(1)} async-done(((bf16[8,64,512]{2,1,0:T(8,128)(2,1)}), bf16[8,64,512]{2,1,0:T(8,128)(2,1)S(1)}, u32[]{:S(2)}, u32[]{:S(2)}) %all-to-all-start.3) | async-done | bytes 524320 | tf_op jit(solution)/shard_map/all_to_all | solution.py:104
  166.3 1.9 gather_fusion
  168.2 1.3 reshape.143
  169.5 0.0 copy-start.5
  169.5 0.0 copy-start.42
  169.5 0.4 fusion.127
  169.9 1.0 fusion.18
  170.9 0.0 copy-start.3
  170.9 10.2 %all_gather.10 = bf16[128,2048]{1,0:T(8,128)(2,1)S(1)} all-gather(bf16[128,512]{1,0:T(8,128)(2,1)S(1)} %fusion.18), channel_id=1, replica_groups=mesh['sp'=8,'tp'=4] {'tp'}, dimensions={1}, use_global_device_ids=true | all-gather | bytes 655360 | tf_op jit(solution)/shard_map/all_gather | solution.py:117
  181.1 1.6 convolution_convert_fusion.3
  182.8 0.0 reduce-scatter.5.cloned.1.call-update
  182.8 5.7 %fusion.2 = bf16[1,704,2048]{2,1,0:T(8,128)(2,1)} fusion(bf16[512,2048]{1,0:T(8,128)(2,1)} %bitcast.94, f32[512,704]{0,1:T(8,128)} %copy-done.48, f32[512,704]{0,1:T(8,128)} %copy-done.47), kind=kOutput, calls=%fused_computation.11 | convolution fusion | flops 1479999488 | bytes 7864320 | tf_op jit(solution)/shard_map/dot_general | solution.py:24
  188.5 2.3 %fusion.125 = (f32[128]{0:T(128)S(1)}, f32[128]{0:T(128)S(1)}, f32[128,256]{1,0:T(8,128)}) fusion(f32[128]{0:T(128)} %param.26, f32[128]{0:T(128)} %param.25, bf16[128,256]{1,0:T(8,128)(2,1)} %param.24, f32[256]{0:T(256)} %param.27, bf16[128,2048]{1,0:T(8,128)(2,1)S(1)} %all_gather.10, bf16[2048,256]{1,0:T(8,128)(2,1)} %all-gather.5.cloned.1.call-done), kind=kOutput, calls=%fused_computation.223 | convolution fusion | flops 134741760 | bytes 1772544 | tf_op jit(solution)/shard_map/dot_general | solution.py:123
  190.8 8.9 %all-reduce = (f32[128]{0:T(128)S(1)}, f32[128]{0:T(128)S(1)}) all-reduce(f32[128]{0:T(128)S(1)} %get-tuple-element.8, f32[128]{0:T(128)S(1)} %get-tuple-element.7), channel_id=1, replica_groups=mesh['sp'=8,'tp'=4] {'tp'}, use_global_device_ids=true, to_apply=%region_10.11 | all-reduce | flops 256 | bytes 2048 | tf_op jit(solution)/shard_map/psum | solution.py:134
  199.8 1.0 subtract_multiply_fusion
  200.8 0.0 copy-start.10
  200.9 0.0 copy-start.11
  201.1 1.3 collective-permute-start
  202.4 5.1 %fusion = bf16[1,704,2048]{2,1,0:T(8,128)(2,1)} fusion(bf16[512,704]{0,1:T(8,128)(2,1)} %copy-done.2, bf16[512,2048]{1,0:T(8,128)(2,1)} %bitcast.137), kind=kOutput, calls=%fused_computation.9 | convolution fusion | flops 1477836800 | bytes 5701632 | tf_op jit(solution)/shard_map/dot_general | solution.py:24
  207.8 1.1 multiply_convert_fusion.6
  208.9 0.7 multiply_convert_fusion.7
  209.6 3.6 %reduce-scatter.5.cloned.1.call-done = bf16[256,256]{1,0:T(8,128)(2,1)} async-done(((bf16[2048,256]{1,0:T(8,128)(2,1)}), bf16[256,256]{1,0:T(8,128)(2,1)}) %reduce-scatter.5.cloned.1.call-update) | async-done | bytes 131088 | tf_op jit(solution)/shard_map/reduce_scatter | solution.py:129
  213.2 1.6 convert_element_type.92
  (100 shorter events, 0.3 us)
Async XLA Ops:
  8.0 89.3 %copy-start = (bf16[1,704,2048]{2,1,0:T(8,128)(2,1)S(1)}, bf16[1,704,2048]{2,1,0:T(8,128)(2,1)}, u32[]{:S(2)}) copy-start(bf16[1,704,2048]{2,1,0:T(8,128)(2,1)} %param.19) | copy-start | bytes 8650756
  8.0 28.8 %copy-start.41 = (f32[128,2]{0,1:T(2,128)S(1)}, f32[128,2]{0,1:T(2,128)}, u32[]{:S(2)}) copy-start(f32[128,2]{0,1:T(2,128)} %param.18) | copy-start | bytes 3076
  8.0 29.0 %copy-start.4 = (bf16[128,512]{1,0:T(8,128)(2,1)S(1)}, bf16[128,512]{1,0:T(8,128)(2,1)}, u32[]{:S(2)}) copy-start(bf16[128,512]{1,0:T(8,128)(2,1)} %param.16) | copy-start | bytes 393220
  8.0 89.2 %all-gather.3.cloned.1.call-start = ((), (), s32[]{:S(2)}) async-start(), calls=%async_computation.6 | async-start | bytes 2621440 | tf_op jit(solution)/shard_map/all_gather | solution.py:73
  36.7 109.7 %reduce-scatter.3.cloned.1.call-start = ((), (), s32[]{:S(2)}) async-start(), calls=%async_computation.7 | async-start | bytes 2621440 | tf_op jit(solution)/shard_map/reduce_scatter | solution.py:100
  97.3 3.4 %copy-start.44 = (bf16[1,704,2048]{2,1,0:T(8,128)(2,1)S(1)}, bf16[1,704,2048]{2,1,0:T(8,128)(2,1)}, u32[]{:S(2)}) copy-start(bf16[1,704,2048]{2,1,0:T(8,128)(2,1)} %param.20) | copy-start | bytes 8650756
  97.3 3.5 %copy-start.45 = (bf16[8,64,2048]{2,1,0:T(8,128)(2,1)S(1)}, bf16[8,64,2048]{2,1,0:T(8,128)(2,1)}, u32[]{:S(2)}) copy-start(bf16[8,64,2048]{2,1,0:T(8,128)(2,1)} %all-gather.3.cloned.1.call-done) | copy-start | bytes 6291460
  100.7 1.7 copy-start.47
  100.7 2.1 copy-start.1
  100.7 3.5 %copy-start.43 = (bf16[1,704,2048]{2,1,0:T(8,128)(2,1)S(1)}, bf16[1,704,2048]{2,1,0:T(8,128)(2,1)}, u32[]{:S(2)}) copy-start(bf16[1,704,2048]{2,1,0:T(8,128)(2,1)} %param.21) | copy-start | bytes 8650756
  102.5 3.9 %copy-start.48 = (f32[512,704]{0,1:T(8,128)}, f32[512,704]{0,1:T(8,128)S(1)}, u32[]{:S(2)}) copy-start(f32[512,704]{0,1:T(8,128)S(1)} %fusion.8) | copy-start | bytes 4325380
  106.4 1.9 copy-start.2
  106.4 1.9 copy-start.46
  111.6 39.7 %copy-start.9 = (bf16[31,256]{1,0:T(8,128)(2,1)S(1)}, bf16[31,256]{1,0:T(8,128)(2,1)}, u32[]{:S(2)}) copy-start(bf16[31,256]{1,0:T(8,128)(2,1)} %param.28) | copy-start | bytes 47620
  111.6 76.9 %all-gather.5.cloned.1.call-start = ((), (), s32[]{:S(2)}) async-start(), calls=%async_computation.9 | async-start | bytes 1179648 | tf_op jit(solution)/shard_map/all_gather | solution.py:125
  146.4 19.9 %all-to-all-start.3 = ((bf16[8,64,512]{2,1,0:T(8,128)(2,1)}), bf16[8,64,512]{2,1,0:T(8,128)(2,1)S(1)}, u32[]{:S(2)}, u32[]{:S(2)}) async-start(bf16[8,64,512]{2,1,0:T(8,128)(2,1)} %bitcast.98), calls=%async_computation.4 | async-start | bytes 1048576 | tf_op jit(solution)/shard_map/all_to_all | solution.py:104
  151.0 62.2 %reduce-scatter.5.cloned.1.call-start = ((), (), s32[]{:S(2)}) async-start(), calls=%async_computation.8 | async-start | bytes 1179648 | tf_op jit(solution)/shard_map/reduce_scatter | solution.py:129
  169.5 11.6 %copy-start.5 = (bf16[128,256]{1,0:T(8,128)(2,1)S(1)}, bf16[128,256]{1,0:T(8,128)(2,1)}, u32[]{:S(2)}) copy-start(bf16[128,256]{1,0:T(8,128)(2,1)} %param.24) | copy-start | bytes 196612
  169.5 11.6 %copy-start.37 = (f32[128]{0:T(128)S(1)}, f32[128]{0:T(128)}, u32[]{:S(2)}) copy-start(f32[128]{0:T(128)} %param.26) | copy-start | bytes 1540
  169.5 11.6 %copy-start.39 = (f32[128]{0:T(128)S(1)}, f32[128]{0:T(128)}, u32[]{:S(2)}) copy-start(f32[128]{0:T(128)} %param.25) | copy-start | bytes 1540
  169.5 11.6 %copy-start.42 = (f32[256]{0:T(256)S(1)}, f32[256]{0:T(256)}, u32[]{:S(2)}) copy-start(f32[256]{0:T(256)} %param.27) | copy-start | bytes 3076
  170.9 17.6 %copy-start.3 = (bf16[128,512]{1,0:T(8,128)(2,1)}, bf16[128,512]{1,0:T(8,128)(2,1)S(1)}, u32[]{:S(2)}) copy-start(bf16[128,512]{1,0:T(8,128)(2,1)S(1)} %fusion.18) | copy-start | bytes 393220
  188.5 11.2 %copy-start.6 = (bf16[128,256]{1,0:T(8,128)(2,1)S(1)}, bf16[128,256]{1,0:T(8,128)(2,1)}, u32[]{:S(2)}) copy-start(bf16[128,256]{1,0:T(8,128)(2,1)} %param.24) | copy-start | bytes 196612
  188.5 11.2 %copy-start.38 = (f32[128]{0:T(128)S(1)}, f32[128]{0:T(128)}, u32[]{:S(2)}) copy-start(f32[128]{0:T(128)} %param.26) | copy-start | bytes 1540
  188.5 11.2 %copy-start.40 = (f32[128]{0:T(128)S(1)}, f32[128]{0:T(128)}, u32[]{:S(2)}) copy-start(f32[128]{0:T(128)} %param.25) | copy-start | bytes 1540
  200.8 6.7 %copy-start.7 = (bf16[128,256]{1,0:T(8,128)(2,1)S(1)}, bf16[128,256]{1,0:T(8,128)(2,1)}, u32[]{:S(2)}) copy-start(bf16[128,256]{1,0:T(8,128)(2,1)} %param.23) | copy-start | bytes 196612
  200.8 6.7 %copy-start.8 = (bf16[128,256]{1,0:T(8,128)(2,1)S(1)}, bf16[128,256]{1,0:T(8,128)(2,1)}, u32[]{:S(2)}) copy-start(bf16[128,256]{1,0:T(8,128)(2,1)} %param.22) | copy-start | bytes 196612
  200.8 6.7 %copy-start.10 = (f32[1,256]{1,0:T(1,128)S(1)}, f32[1,256]{1,0:T(1,128)}, u32[]{:S(2)}) copy-start(f32[1,256]{1,0:T(1,128)} %get-tuple-element.40) | copy-start | bytes 3076
  200.9 6.7 %copy-start.11 = (f32[1,256]{1,0:T(1,128)S(1)}, f32[1,256]{1,0:T(1,128)}, u32[]{:S(2)}) copy-start(f32[1,256]{1,0:T(1,128)} %get-tuple-element.41) | copy-start | bytes 3076
  200.9 6.7 %copy-start.12 = (f32[1,256]{1,0:T(1,128)S(1)}, f32[1,256]{1,0:T(1,128)}, u32[]{:S(2)}) copy-start(f32[1,256]{1,0:T(1,128)} %get-tuple-element.42) | copy-start | bytes 3076
  200.9 6.7 %copy-start.13 = (f32[1,256]{1,0:T(1,128)S(1)}, f32[1,256]{1,0:T(1,128)}, u32[]{:S(2)}) copy-start(f32[1,256]{1,0:T(1,128)} %get-tuple-element.43) | copy-start | bytes 3076
  200.9 6.7 %copy-start.14 = (f32[1,256]{1,0:T(1,128)S(1)}, f32[1,256]{1,0:T(1,128)}, u32[]{:S(2)}) copy-start(f32[1,256]{1,0:T(1,128)} %get-tuple-element.44) | copy-start | bytes 3076
  200.9 6.7 %copy-start.15 = (f32[1,256]{1,0:T(1,128)S(1)}, f32[1,256]{1,0:T(1,128)}, u32[]{:S(2)}) copy-start(f32[1,256]{1,0:T(1,128)} %get-tuple-element.45) | copy-start | bytes 3076
  200.9 6.7 %copy-start.16 = (f32[1,256]{1,0:T(1,128)S(1)}, f32[1,256]{1,0:T(1,128)}, u32[]{:S(2)}) copy-start(f32[1,256]{1,0:T(1,128)} %get-tuple-element.46) | copy-start | bytes 3076
  200.9 6.7 %copy-start.17 = (f32[1,256]{1,0:T(1,128)S(1)}, f32[1,256]{1,0:T(1,128)}, u32[]{:S(2)}) copy-start(f32[1,256]{1,0:T(1,128)} %get-tuple-element.47) | copy-start | bytes 3076
  200.9 6.7 %copy-start.18 = (f32[1,256]{1,0:T(1,128)S(1)}, f32[1,256]{1,0:T(1,128)}, u32[]{:S(2)}) copy-start(f32[1,256]{1,0:T(1,128)} %get-tuple-element.17) | copy-start | bytes 3076
  200.9 6.7 %copy-start.19 = (f32[1,256]{1,0:T(1,128)S(1)}, f32[1,256]{1,0:T(1,128)}, u32[]{:S(2)}) copy-start(f32[1,256]{1,0:T(1,128)} %get-tuple-element.18) | copy-start | bytes 3076
  201.0 6.7 %copy-start.20 = (f32[1,256]{1,0:T(1,128)S(1)}, f32[1,256]{1,0:T(1,128)}, u32[]{:S(2)}) copy-start(f32[1,256]{1,0:T(1,128)} %get-tuple-element.19) | copy-start | bytes 3076
  201.0 6.7 %copy-start.21 = (f32[1,256]{1,0:T(1,128)S(1)}, f32[1,256]{1,0:T(1,128)}, u32[]{:S(2)}) copy-start(f32[1,256]{1,0:T(1,128)} %get-tuple-element.20) | copy-start | bytes 3076
  201.0 6.7 %copy-start.22 = (f32[1,256]{1,0:T(1,128)S(1)}, f32[1,256]{1,0:T(1,128)}, u32[]{:S(2)}) copy-start(f32[1,256]{1,0:T(1,128)} %get-tuple-element.21) | copy-start | bytes 3076
  201.0 6.7 %copy-start.23 = (f32[1,256]{1,0:T(1,128)S(1)}, f32[1,256]{1,0:T(1,128)}, u32[]{:S(2)}) copy-start(f32[1,256]{1,0:T(1,128)} %get-tuple-element.22) | copy-start | bytes 3076
  201.0 6.7 %copy-start.24 = (f32[1,256]{1,0:T(1,128)S(1)}, f32[1,256]{1,0:T(1,128)}, u32[]{:S(2)}) copy-start(f32[1,256]{1,0:T(1,128)} %get-tuple-element.23) | copy-start | bytes 3076
  201.0 6.7 %copy-start.25 = (f32[1,256]{1,0:T(1,128)S(1)}, f32[1,256]{1,0:T(1,128)}, u32[]{:S(2)}) copy-start(f32[1,256]{1,0:T(1,128)} %get-tuple-element.24) | copy-start | bytes 3076
  201.0 6.7 %copy-start.26 = (f32[1,256]{1,0:T(1,128)S(1)}, f32[1,256]{1,0:T(1,128)}, u32[]{:S(2)}) copy-start(f32[1,256]{1,0:T(1,128)} %get-tuple-element.25) | copy-start | bytes 3076
  201.0 6.7 %copy-start.27 = (f32[1,256]{1,0:T(1,128)S(1)}, f32[1,256]{1,0:T(1,128)}, u32[]{:S(2)}) copy-start(f32[1,256]{1,0:T(1,128)} %get-tuple-element.26) | copy-start | bytes 3076
  201.0 6.7 %copy-start.28 = (f32[1,256]{1,0:T(1,128)S(1)}, f32[1,256]{1,0:T(1,128)}, u32[]{:S(2)}) copy-start(f32[1,256]{1,0:T(1,128)} %get-tuple-element.27) | copy-start | bytes 3076
  201.0 6.7 %copy-start.29 = (f32[1,256]{1,0:T(1,128)S(1)}, f32[1,256]{1,0:T(1,128)}, u32[]{:S(2)}) copy-start(f32[1,256]{1,0:T(1,128)} %get-tuple-element.28) | copy-start | bytes 3076
  201.1 6.7 %copy-start.30 = (f32[1,256]{1,0:T(1,128)S(1)}, f32[1,256]{1,0:T(1,128)}, u32[]{:S(2)}) copy-start(f32[1,256]{1,0:T(1,128)} %get-tuple-element.29) | copy-start | bytes 3076
  201.1 6.7 %copy-start.31 = (f32[1,256]{1,0:T(1,128)S(1)}, f32[1,256]{1,0:T(1,128)}, u32[]{:S(2)}) copy-start(f32[1,256]{1,0:T(1,128)} %get-tuple-element.30) | copy-start | bytes 3076
  201.1 6.7 %copy-start.32 = (f32[1,256]{1,0:T(1,128)S(1)}, f32[1,256]{1,0:T(1,128)}, u32[]{:S(2)}) copy-start(f32[1,256]{1,0:T(1,128)} %get-tuple-element.31) | copy-start | bytes 3076
  201.1 6.7 %copy-start.33 = (f32[1,256]{1,0:T(1,128)S(1)}, f32[1,256]{1,0:T(1,128)}, u32[]{:S(2)}) copy-start(f32[1,256]{1,0:T(1,128)} %get-tuple-element.32) | copy-start | bytes 3076
  201.1 6.7 %copy-start.34 = (f32[1,256]{1,0:T(1,128)S(1)}, f32[1,256]{1,0:T(1,128)}, u32[]{:S(2)}) copy-start(f32[1,256]{1,0:T(1,128)} %get-tuple-element.33) | copy-start | bytes 3076
  201.1 6.7 %copy-start.35 = (f32[1,256]{1,0:T(1,128)S(1)}, f32[1,256]{1,0:T(1,128)}, u32[]{:S(2)}) copy-start(f32[1,256]{1,0:T(1,128)} %get-tuple-element.34) | copy-start | bytes 3076
  201.1 6.7 %copy-start.36 = (f32[1,256]{1,0:T(1,128)S(1)}, f32[1,256]{1,0:T(1,128)}, u32[]{:S(2)}) copy-start(f32[1,256]{1,0:T(1,128)} %get-tuple-element.35) | copy-start | bytes 3076
  201.1 6.4 %collective-permute-start = (f32[30,256]{1,0:T(8,128)S(1)}, f32[30,256]{1,0:T(8,128)S(1)}, u32[]{:S(2)}, u32[]{:S(2)}) collective-permute-start(f32[30,256]{1,0:T(8,128)S(1)} %slice.274), channel_id=1, source_target_pairs={{4,0},{8,4},{12,8},{16,12},{20,16},{24,20},{28,24},{5,1},{9,5},{13... | collective-permute-start | bytes 92168 | tf_op jit(solution)/shard_map/ppermute | solution.py:10
Sparse Core Ops, SparseCore 0:
  36.9 47.4 all-gather.2
  111.7 34.6 reduce-scatter.2
Sparse Core Ops, SparseCore 1:
  113.7 21.6 all-gather.4
  182.9 30.3 reduce-scatter.4
